TPU v7x, 32 devices: a whole 2x2x4 slice. The times are simulated.
32 devices in a mesh: ep: 8 (over z, y), tp: 4 (over x, core).
Axes of the slice: x: 2, y: 2, z: 4, core: 2. Of those that a mesh axis runs over, the one named last changes fastest.
Arguments:
- tokens: bfloat16 [256, 2048], P('ep'), may hold values from -6 to 6
- gain_mix: bfloat16 [2048], replicated, may hold values from 0.099609375 to 1.8984375
- gain_ffn: bfloat16 [2048], replicated, may hold values from 0.099609375 to 1.8984375
- w_query: bfloat16 [2048, 1024], P('ep', 'tp'), may hold values from -0.125 to 0.125
- w_key: bfloat16 [2048, 1024], P('ep', 'tp'), may hold values from -0.125 to 0.125
- w_value: bfloat16 [2048, 1024], P('ep', 'tp'), may hold values from -0.125 to 0.125
- w_outgate: bfloat16 [2048, 1024], P('ep', 'tp'), may hold values from -0.125 to 0.125
- w_ingate: bfloat16 [2048, 8], replicated, may hold values from -0.125 to 0.125
- w_forget: bfloat16 [2048, 8], replicated, may hold values from -0.125 to 0.125
- bias_in: float32 [8], replicated, may hold values from -2 to 2
- bias_forget: float32 [8], replicated, may hold values from -1 to 3
- w_proj: bfloat16 [1024, 2048], P('tp'), may hold values from -0.1875 to 0.1875
- matrix_state: float32 [256, 8, 128, 128], P('ep', 'tp'), may hold values from -0.6 to 0.6
- normal_state: float32 [256, 8, 128], P('ep', 'tp'), may hold values from -0.6 to 0.6
- stab_state: float32 [256, 8], P('ep', 'tp'), may hold values from -1 to 1
- route_ids: int32 [256, 2], P('ep'), may hold values from 0 to 3, all different within a row; in each aligned block of 32 rows (0 to 31, 32 to 63, ...) at most 32 rows name the same one
- route_weights: float32 [256, 2], P('ep'), may hold values from 0.1 to 1
- w_exp_gate: bfloat16 [8, 2048, 1536], P('ep', None, 'tp'), may hold values from -0.125 to 0.125
- w_exp_up: bfloat16 [8, 2048, 1536], P('ep', None, 'tp'), may hold values from -0.125 to 0.125
- w_exp_down: bfloat16 [8, 1536, 2048], P('ep', 'tp'), may hold values from -0.109375 to 0.109375
Outputs:
- mixed_out: bfloat16 [256, 2048], P('ep', 'tp')
- matrix_out: float32 [256, 8, 128, 128], P('ep', 'tp')
- normal_out: float32 [256, 8, 128], P('ep', 'tp')
- stab_out: float32 [256, 8], P('ep', 'tp')
Inputs may be any that keep to these rules, and one draw needn't show every extreme that they name: `route_ids`: each row names 2 different experts; among the rows of one index of ep no expert is named by more than 32 rows, and in every draw some expert is named by exactly 32 of them.
All inputs are finite; a program needn't handle non-finite values.
Results may differ from a plain program's by a relative error of at most 0.015.
Values may be sent and summed in bfloat16 or wider, within the bound.
No kernel may reach another device: no remote copies, remote signals or barrier semaphores. Data moves between devices by JAX's collectives and lax.ppermute only.
A program may use at most 64 MiB of HBM per device.

v0:
```python
import jax
import jax.numpy as jnp
from jax import lax
from jax.sharding import PartitionSpec as P

norm_epsilon = 1e-06


def rms_scale(row_block, gain):
    wide = row_block.astype(jnp.float32)
    factor = lax.rsqrt(jnp.mean(wide * wide, axis=-1, keepdims=True) + norm_epsilon)
    return (wide * factor * gain.astype(jnp.float32)).astype(jnp.bfloat16)


def memory_step(
    query,
    key_rows,
    value_rows,
    gate_rows,
    in_pre,
    forget_pre,
    matrix_state,
    normal_state,
    stab_state,
):
    log_forget = jax.nn.log_sigmoid(forget_pre)
    stab_new = jnp.maximum(log_forget + stab_state, in_pre)
    carry = jnp.exp(log_forget + stab_state - stab_new)
    inflow = jnp.exp(in_pre - stab_new)
    scaled_keys = key_rows.astype(jnp.float32) * query.shape[-1] ** (-0.5)
    value_wide = value_rows.astype(jnp.float32)
    matrix_new = (
        carry[..., None, None] * matrix_state
        + inflow[..., None, None] * scaled_keys[..., :, None] * value_wide[..., None, :]
    )
    normal_new = carry[..., None] * normal_state + inflow[..., None] * scaled_keys
    query_wide = query.astype(jnp.float32)
    numer = jnp.einsum("shd,shde->she", query_wide, matrix_new, precision=lax.Precision.HIGHEST)
    denom = jnp.maximum(jnp.abs(jnp.sum(query_wide * normal_new, axis=-1)), 1.0)
    hidden = numer / denom[..., None] * jax.nn.sigmoid(gate_rows.astype(jnp.float32))
    return (hidden, matrix_new, normal_new, stab_new)


def dispatch_table(route_ids, experts, capacity):
    flat_ids = route_ids.reshape(-1)
    expert_hot = (flat_ids[:, None] == jnp.arange(experts, dtype=jnp.int32)[None, :]).astype(
        jnp.int32
    )
    slot_rank = jnp.sum((jnp.cumsum(expert_hot, axis=0) - 1) * expert_hot, axis=1)
    slot_hot = (slot_rank[:, None] == jnp.arange(capacity, dtype=jnp.int32)[None, :]).astype(
        jnp.float32
    )
    table = expert_hot.astype(jnp.float32)[:, :, None] * slot_hot[:, None, :]
    return table.reshape(flat_ids.shape[0], experts * capacity)


def pack_rows(table, row_block, top_count, experts, capacity):
    repeated = jnp.repeat(row_block, top_count, axis=0)
    packed = jnp.einsum(
        "as,aw->sw", table.astype(jnp.bfloat16), repeated, preferred_element_type=jnp.float32
    ).astype(jnp.bfloat16)
    return packed.reshape(experts, capacity, row_block.shape[1])


def swap(value, axis, bit):
    count = lax.axis_size(axis)
    return lax.ppermute(value, axis, [(i, i ^ bit) for i in range(count)])


def bits_of(count):
    return [1 << place for place in range(count.bit_length() - 1)]


def scatter_columns(terms, axis):
    count = lax.axis_size(axis)
    index = lax.axis_index(axis)
    width = terms.shape[1] // count

    def block(peer):
        return lax.dynamic_slice_in_dim(terms, (index ^ peer) * width, width, 1)

    total = block(0)
    for peer in range(1, count):
        total = total + swap(block(peer).astype(jnp.bfloat16), axis, peer).astype(jnp.float32)
    return total


def halve_columns(terms, axis):
    count = lax.axis_size(axis)
    index = lax.axis_index(axis)
    rows, columns = terms.shape
    blocks = terms.reshape(rows, count, columns // count)
    for bit in bits_of(count):
        pairs = blocks.reshape(rows, -1, 2, blocks.shape[-1])
        own = index // bit % 2
        kept = jnp.where(own == 0, pairs[:, :, 0], pairs[:, :, 1])
        sent = jnp.where(own == 0, pairs[:, :, 1], pairs[:, :, 0]).astype(jnp.bfloat16)
        blocks = kept + swap(sent, axis, bit).astype(jnp.float32)
    return blocks.reshape(rows, columns // count)


def gather_columns(own, axis):
    count = lax.axis_size(axis)
    index = lax.axis_index(axis)
    held = own[None]
    for bit in reversed(bits_of(count)):
        other = swap(held, axis, bit)
        first = index // bit % 2 == 0
        low = jnp.where(first, held, other)
        high = jnp.where(first, other, held)
        held = jnp.stack([low, high], axis=1).reshape((-1,) + own.shape)
    return held


def body(
    tokens,
    gain_mix,
    gain_ffn,
    w_query,
    w_key,
    w_value,
    w_outgate,
    w_ingate,
    w_forget,
    bias_in,
    bias_forget,
    w_proj,
    matrix_state,
    normal_state,
    stab_state,
    route_ids,
    route_weights,
    w_exp_gate,
    w_exp_up,
    w_exp_down,
):
    ep_count = lax.axis_size("ep")
    tp_count = lax.axis_size("tp")
    ep_index = lax.axis_index("ep")
    tp_index = lax.axis_index("tp")
    seq_dev = tokens.shape[0]
    model_width = tokens.shape[1]
    heads_dev = matrix_state.shape[1]
    head_dim = matrix_state.shape[2]
    head_cols = w_query.shape[1]
    feature_rows = w_query.shape[0]
    top_count = route_ids.shape[1]
    experts = ep_count // 2
    capacity = min(seq_dev, max(2, 2 * seq_dev * top_count // experts))
    every_row = capacity == seq_dev
    col_width = model_width // tp_count
    foreign = lax.all_to_all(tokens, "ep", split_axis=1, concat_axis=0, tiled=True)
    own_gain = lax.dynamic_slice_in_dim(gain_mix, ep_index * feature_rows, feature_rows, 0)
    scaled = (foreign.astype(jnp.float32) * own_gain.astype(jnp.float32)).astype(jnp.bfloat16)
    terms = jnp.concatenate(
        [
            jnp.dot(scaled, weight, preferred_element_type=jnp.float32).astype(jnp.bfloat16)
            for weight in (w_query, w_key, w_value, w_outgate)
        ],
        axis=1,
    )
    arrived = lax.all_to_all(terms, "ep", split_axis=0, concat_axis=0, tiled=True)
    wide = tokens.astype(jnp.float32)
    factor = lax.rsqrt(jnp.mean(wide * wide, axis=-1, keepdims=True) + norm_epsilon)
    summed = factor * jnp.sum(
        arrived.astype(jnp.float32).reshape(ep_count, seq_dev, 4 * head_cols), axis=0
    )
    query, key_rows, value_rows, gate_rows = [
        summed[:, offset * head_cols : (offset + 1) * head_cols]
        .astype(jnp.bfloat16)
        .reshape(seq_dev, heads_dev, head_dim)
        for offset in range(4)
    ]
    normed = (wide * factor * gain_mix.astype(jnp.float32)).astype(jnp.bfloat16)
    head_first = tp_index * heads_dev
    in_pre = lax.dynamic_slice_in_dim(
        jnp.dot(normed, w_ingate, preferred_element_type=jnp.float32) + bias_in,
        head_first,
        heads_dev,
        1,
    )
    forget_pre = lax.dynamic_slice_in_dim(
        jnp.dot(normed, w_forget, preferred_element_type=jnp.float32) + bias_forget,
        head_first,
        heads_dev,
        1,
    )
    hidden, matrix_new, normal_new, stab_new = memory_step(
        query,
        key_rows,
        value_rows,
        gate_rows,
        in_pre,
        forget_pre,
        matrix_state,
        normal_state,
        stab_state,
    )
    cell = hidden.reshape(seq_dev, head_cols).astype(jnp.bfloat16)
    partial_out = jnp.dot(cell, w_proj, preferred_element_type=jnp.float32)
    own_tokens = lax.dynamic_slice_in_dim(tokens, tp_index * col_width, col_width, 1)
    attended = scatter_columns(partial_out, "tp")
    own_resid = (own_tokens.astype(jnp.float32) + attended).astype(jnp.bfloat16)
    if every_row:
        packed = jnp.broadcast_to(own_resid, (experts, seq_dev, col_width))
    else:
        table = dispatch_table(route_ids, experts, capacity)
        packed = pack_rows(table, own_resid, top_count, experts, capacity)
    outgoing = jnp.broadcast_to(packed[:, None], (experts, 2, capacity, col_width))
    received = lax.all_to_all(
        outgoing.reshape(ep_count * capacity, col_width),
        "ep",
        split_axis=0,
        concat_axis=0,
        tiled=True,
    )
    rows = gather_columns(received, "tp").transpose(1, 0, 2).reshape(-1, model_width)
    normed_ffn = rms_scale(rows, gain_ffn)
    gate_sum = jnp.dot(normed_ffn, w_exp_gate[0], preferred_element_type=jnp.float32)
    up_sum = jnp.dot(normed_ffn, w_exp_up[0], preferred_element_type=jnp.float32)
    inner = (jax.nn.silu(gate_sum) * up_sum).astype(jnp.bfloat16)
    expert_terms = jnp.dot(inner, w_exp_down[0], preferred_element_type=jnp.float32)
    half_share = halve_columns(expert_terms, "tp").astype(jnp.bfloat16)
    returned = lax.all_to_all(half_share, "ep", split_axis=0, concat_axis=0, tiled=True)
    halves = returned.astype(jnp.float32).reshape(experts, 2, capacity, col_width)
    weights = route_weights / jnp.sum(route_weights, axis=-1, keepdims=True)
    if every_row:
        chosen = route_ids[:, :, None] == jnp.arange(experts, dtype=jnp.int32)
        shares = jnp.sum(jnp.where(chosen, weights[:, :, None], 0.0), axis=1)
        routed = jnp.sum(halves * shares.T[:, None, :, None], axis=(0, 1))
    else:
        combine = jnp.sum(
            (table * weights.reshape(-1)[:, None]).reshape(seq_dev, top_count, experts * capacity),
            axis=1,
        )
        halves_summed = jnp.sum(halves, axis=1).reshape(experts * capacity, col_width)
        routed = jnp.dot(combine, halves_summed, precision=lax.Precision.HIGHEST)
    mixed_out = (own_resid.astype(jnp.float32) + routed).astype(jnp.bfloat16)
    return (mixed_out, matrix_new, normal_new, stab_new)


def solution(mesh):
    placed = (
        P("ep", None),
        P(),
        P(),
        P("ep", "tp"),
        P("ep", "tp"),
        P("ep", "tp"),
        P("ep", "tp"),
        P(),
        P(),
        P(),
        P(),
        P("tp", None),
        P("ep", "tp", None, None),
        P("ep", "tp", None),
        P("ep", "tp"),
        P("ep", None),
        P("ep", None),
        P("ep", None, "tp"),
        P("ep", None, "tp"),
        P("ep", "tp", None),
    )
    return jax.shard_map(
        body,
        mesh=mesh,
        in_specs=placed,
        out_specs=(P("ep", "tp"), P("ep", "tp", None, None), P("ep", "tp", None), P("ep", "tp")),
        check_vma=False,
    )
```

profile of v0, /device:TPU:0, one launch (start us, length us, event | category | flops | bytes accessed | tf_op | source)
XLA Modules:
  0.0 111.9 jit_solution(5496403255579965468)
XLA Ops:
  0.7 1.7 %copy.99 = bf16[4,8,8,256]{3,2,0,1:T(8,128)(2,1)} copy(bf16[4,8,8,256]{3,2,1,0:T(8,128)(2,1)} %bitcast.125) | data formatting | bytes 262144 | tf_op jit(solution)/shard_map/all_to_all | solution.py:152
  2.4 7.3 %all-to-all-start = ((bf16[32,8,256]{2,0,1:T(8,128)(2,1)}), bf16[32,8,256]{2,0,1:T(8,128)(2,1)S(1)}, u32[]{:S(2)}, u32[]{:S(2)}) async-start(bf16[32,8,256]{2,0,1:T(8,128)(2,1)} %bitcast.117), calls=%async_computation | async-start | bytes 262144 | tf_op jit(solution)/shard_map/all_to_all | solution.py:152
  11.5 5.6 %all-to-all-done = bf16[32,8,256]{2,0,1:T(8,128)(2,1)S(1)} async-done(((bf16[32,8,256]{2,0,1:T(8,128)(2,1)}), bf16[32,8,256]{2,0,1:T(8,128)(2,1)S(1)}, u32[]{:S(2)}, u32[]{:S(2)}) %all-to-all-start) | async-done | bytes 131104 | tf_op jit(solution)/shard_map/all_to_all | solution.py:152
  18.2 1.2 %convolution_convert_fusion.1 = bf16[256,256]{0,1:T(8,128)(2,1)S(1)} fusion(bf16[256,256]{1,0:T(8,128)(2,1)S(1)} %fusion.34, bf16[256,256]{1,0:T(8,128)(2,1)} %param.25), kind=kOutput, calls=%fused_computation.14 | convolution fusion | flops 33619968 | bytes 393216 | tf_op jit(solution)/shard_map/dot_general | solution.py:157
  19.5 1.1 %convolution_convert_fusion.2 = bf16[256,256]{0,1:T(8,128)(2,1)S(1)} fusion(bf16[256,256]{1,0:T(8,128)(2,1)S(1)} %fusion.34, bf16[256,256]{1,0:T(8,128)(2,1)} %param.24), kind=kOutput, calls=%fused_computation.15 | convolution fusion | flops 33619968 | bytes 393216 | tf_op jit(solution)/shard_map/dot_general | solution.py:157
  21.9 3.5 %all-to-all-start.1 = ((bf16[8,32,1024]{2,1,0:T(8,128)(2,1)}), bf16[8,32,1024]{2,1,0:T(8,128)(2,1)S(1)}, u32[]{:S(2)}, u32[]{:S(2)}) async-start(bf16[8,32,1024]{2,1,0:T(8,128)(2,1)} %bitcast.2), calls=%async_computation.1 | async-start | bytes 1048576 | tf_op jit(solution)/shard_map/all_to_all | solution.py:162
  26.2 12.5 %all-to-all-done.1 = bf16[8,32,1024]{2,1,0:T(8,128)(2,1)S(1)} async-done(((bf16[8,32,1024]{2,1,0:T(8,128)(2,1)}), bf16[8,32,1024]{2,1,0:T(8,128)(2,1)S(1)}, u32[]{:S(2)}, u32[]{:S(2)}) %all-to-all-start.1) | async-done | bytes 524320 | tf_op jit(solution)/shard_map/all_to_all | solution.py:162
  39.8 3.7 %multiply_add_fusion = f32[32,2,128,128]{3,2,1,0:T(8,128)S(1)} fusion(f32[32,2,128,128]{3,2,1,0:T(8,128)} %param.32, f32[32,2,128]{2,1,0:T(2,128)S(1)} %reshape.185, f32[32,2,128]{2,1,0:T(2,128)S(1)} %get-tuple-element.6, f32[32,2]{1,0:T(8,128)S(1)} %copy.77), kind=kLoop, calls=%fused_computation | loop fusion | flops 3145728 | bytes 8454400 | tf_op jit(solution)/shard_map/add | solution.py:33
  43.5 2.0 %fusion.48 = f32[32,2,1,128]{3,2,1,0:T(1,128)S(1)} fusion(bf16[32,2,128,1]{2,3,1,0:T(2,128)(2,1)S(1)} %reshape.194, f32[32,2,128,128]{3,2,1,0:T(8,128)S(1)} %multiply_add_fusion), kind=kOutput, calls=%fused_computation.88 | convolution fusion | flops 12582912 | bytes 4243456 | tf_op jit(solution)/shard_map/shd,shde->she/dot_general | solution.py:38
  46.1 1.6 %collective-permute-start.1 = (bf16[32,512]{1,0:T(8,128)(2,1)S(1)}, bf16[32,512]{1,0:T(8,128)(2,1)S(1)}, u32[]{:S(2)}, u32[]{:S(2)}) collective-permute-start(bf16[32,512]{1,0:T(8,128)(2,1)S(1)} %get-tuple-element.15), channel_id=1, source_target_pairs={{0,2},{1,3},{2,0},{3,1},{4,6},{5,7},{6,4},{7,5},{8,10},{9,11},{10,... | collective-permute-start | bytes 98312 | tf_op jit(solution)/shard_map/ppermute | solution.py:67
  47.9 2.1 %collective-permute-done.1 = bf16[32,512]{1,0:T(8,128)(2,1)S(1)} collective-permute-done((bf16[32,512]{1,0:T(8,128)(2,1)S(1)}, bf16[32,512]{1,0:T(8,128)(2,1)S(1)}, u32[]{:S(2)}, u32[]{:S(2)}) %collective-permute-start.1) | collective-permute-done | bytes 32800 | tf_op jit(solution)/shard_map/ppermute | solution.py:67
  51.0 12.7 %all_to_all.37 = bf16[8,32,512]{2,1,0:T(8,128)(2,1)S(1)} all-to-all(bf16[8,32,512]{2,1,0:T(8,128)(2,1)S(1)} %all_to_all.30), channel_id=1, replica_groups=mesh['ep'=8,'tp'=4] {'ep'}, dimensions={0} | all-to-all | bytes 524288 | tf_op jit(solution)/shard_map/all_to_all | solution.py:210
  64.6 5.7 %collective-permute-done.3 = bf16[1,256,512]{2,1,0:T(8,128)(2,1)S(1)} collective-permute-done((bf16[1,256,512]{2,1,0:T(8,128)(2,1)S(1)}, bf16[1,256,512]{2,1,0:T(8,128)(2,1)S(1)}, u32[]{:S(2)}, u32[]{:S(2)}) %collective-permute-start.3) | collective-permute-done | bytes 262176 | tf_op jit(solution)/shard_map/ppermute | solution.py:67
  70.5 2.6 %copy.90 = bf16[2048,384]{1,0:T(8,128)(2,1)} copy(bf16[2048,384]{0,1:T(8,128)(2,1)} %bitcast.121) | data formatting | bytes 3145728 | tf_op jit(solution)/shard_map/dot_general | solution.py:222
  73.6 1.3 %fusion.16 = bf16[256,4,512]{2,0,1:T(8,128)(2,1)} fusion(bf16[2,2,256,512]{3,2,1,0:T(8,128)(2,1)S(1)} %pad_maximum_fusion, f32[4,512]{1,0:T(4,128)S(1)} %reshape.189, f32[256]{0:T(256)S(1)} %add_rsqrt_fusion), kind=kLoop, calls=%fused_computation.19 | loop fusion | flops 2097152 | bytes 2106368 | tf_op jit(solution)/shard_map/convert_element_type | solution.py:12
  74.9 1.5 %copy.81 = bf16[256,4,512]{0,2,1:T(8,128)(2,1)S(1)} copy(bf16[256,4,512]{2,0,1:T(8,128)(2,1)} %fusion.16) | data formatting | bytes 2097152 | tf_op jit(solution)/shard_map/convert_element_type | solution.py:12
  76.4 2.1 %fusion.5 = f32[256,384]{1,0:T(8,128)S(1)} fusion(bf16[256,2048]{0,1:T(8,128)(2,1)S(1)} %bitcast.119, bf16[1,2048,384]{2,1,0:T(8,128)(2,1)} %param.37), kind=kOutput, calls=%fused_computation.8 | convolution fusion | flops 402653184 | bytes 3014656 | tf_op jit(solution)/shard_map/dot_general | solution.py:219
  78.6 4.1 %fusion.21 = f32[256,2,2,512]{3,0,2,1:T(8,128)} fusion(bf16[2,2,512,384]{3,2,1,0:T(8,128)(2,1)} %bitcast.122, bf16[256,2048]{0,1:T(8,128)(2,1)S(1)} %bitcast.120, bf16[1,2048,384]{2,1,0:T(8,128)(2,1)S(1)} %copy-done, f32[256,384]{1,0:T(8,128)S(1)} %fusion.5), kind=kOutput, calls=%fused_computation.27 | convolution fusion | flops 805896192 | bytes 6684672 | tf_op jit(solution)/shard_map/dot_general | solution.py:222
  82.7 1.6 %fusion.23 = bf16[256,2,512]{2,0,1:T(8,128)(2,1)S(1)} fusion(f32[256,2,2,512]{3,0,2,1:T(8,128)} %fusion.21, pred[]{:T(512)S(6)} %eq.29), kind=kLoop, calls=%fused_computation.28 | loop fusion | flops 262144 | bytes 1572865 | tf_op jit(solution)/shard_map/convert_element_type | solution.py:97
  84.9 1.5 %collective-permute-done.5 = bf16[256,2,512]{2,0,1:T(8,128)(2,1)S(1)} collective-permute-done((bf16[256,2,512]{2,0,1:T(8,128)(2,1)S(1)}, bf16[256,2,512]{2,0,1:T(8,128)(2,1)S(1)}, u32[]{:S(2)}, u32[]{:S(2)}) %collective-permute-start.5) | collective-permute-done | bytes 524320 | tf_op jit(solution)/shard_map/ppermute | solution.py:67
  86.4 1.8 %fusion.19 = f32[256,1,2,512]{3,0,2,1:T(8,128)S(1)} fusion(bf16[256,2,512]{2,0,1:T(8,128)(2,1)S(1)} %collective-permute-done.5, f32[256,2,2,512]{3,0,2,1:T(8,128)} %fusion.21, pred[]{:T(512)S(6)} %eq.29), kind=kLoop, calls=%fused_computation.24 | loop fusion | flops 786432 | bytes 3670017 | tf_op jit(solution)/shard_map/reshape | solution.py:94
  89.3 7.7 %collective-permute-done.6 = bf16[256,1,512]{2,0,1:T(8,128)(2,1)S(1)} collective-permute-done((bf16[256,1,512]{2,0,1:T(8,128)(2,1)S(1)}, bf16[256,1,512]{2,0,1:T(8,128)(2,1)S(1)}, u32[]{:S(2)}, u32[]{:S(2)}) %collective-permute-start.6) | collective-permute-done | bytes 262176 | tf_op jit(solution)/shard_map/ppermute | solution.py:67
  97.8 4.7 %all-to-all-start.3 = ((bf16[8,32,512]{2,1,0:T(8,128)(2,1)}), bf16[8,32,512]{2,1,0:T(8,128)(2,1)S(1)}, u32[]{:S(2)}, u32[]{:S(2)}) async-start(bf16[8,32,512]{2,1,0:T(8,128)(2,1)} %bitcast.31), calls=%async_computation.3 | async-start | bytes 524288 | tf_op jit(solution)/shard_map/all_to_all | solution.py:224
  102.6 8.5 %all-to-all-done.3 = bf16[8,32,512]{2,1,0:T(8,128)(2,1)S(1)} async-done(((bf16[8,32,512]{2,1,0:T(8,128)(2,1)}), bf16[8,32,512]{2,1,0:T(8,128)(2,1)S(1)}, u32[]{:S(2)}, u32[]{:S(2)}) %all-to-all-start.3) | async-done | bytes 262176 | tf_op jit(solution)/shard_map/all_to_all | solution.py:224
  (87 shorter events, 12.5 us)
Async XLA Ops:
  0.6 77.9 %copy-start = (bf16[1,2048,384]{2,1,0:T(8,128)(2,1)S(1)}, bf16[1,2048,384]{2,1,0:T(8,128)(2,1)}, u32[]{:S(2)}) copy-start(bf16[1,2048,384]{2,1,0:T(8,128)(2,1)} %param.38) | copy-start | bytes 4718596
  0.6 20.0 %copy-start.4 = (bf16[256,256]{1,0:T(8,128)(2,1)S(1)}, bf16[256,256]{1,0:T(8,128)(2,1)}, u32[]{:S(2)}) copy-start(bf16[256,256]{1,0:T(8,128)(2,1)} %param.23) | copy-start | bytes 393220
  2.4 14.7 %all-to-all-start = ((bf16[32,8,256]{2,0,1:T(8,128)(2,1)}), bf16[32,8,256]{2,0,1:T(8,128)(2,1)S(1)}, u32[]{:S(2)}, u32[]{:S(2)}) async-start(bf16[32,8,256]{2,0,1:T(8,128)(2,1)} %bitcast.117), calls=%async_computation | async-start | bytes 262144 | tf_op jit(solution)/shard_map/all_to_all | solution.py:152
  18.2 7.3 %copy-start.6 = (bf16[2048]{0:T(1024)(128)(2,1)S(1)}, bf16[2048]{0:T(1024)(128)(2,1)}, u32[]{:S(2)}) copy-start(bf16[2048]{0:T(1024)(128)(2,1)} %param.21) | copy-start | bytes 12292
  18.2 7.3 %copy-start.3 = (bf16[32,2048]{1,0:T(8,128)(2,1)S(1)}, bf16[32,2048]{1,0:T(8,128)(2,1)}, u32[]{:S(2)}) copy-start(bf16[32,2048]{1,0:T(8,128)(2,1)} %param.20) | copy-start | bytes 393220
  18.2 7.3 %copy-start.12 = (bf16[2048,8]{0,1:T(8,128)(2,1)S(1)}, bf16[2048,8]{0,1:T(8,128)(2,1)}, u32[]{:S(2)}) copy-start(bf16[2048,8]{0,1:T(8,128)(2,1)} %param.27) | copy-start | bytes 98308
  18.2 7.3 %copy-start.14 = (f32[8]{0:T(128)S(1)}, f32[8]{0:T(128)}, u32[]{:S(2)}) copy-start(f32[8]{0:T(128)} %param.29) | copy-start | bytes 100
  19.4 6.3 %copy-start.13 = (bf16[2048,8]{0,1:T(8,128)(2,1)S(1)}, bf16[2048,8]{0,1:T(8,128)(2,1)}, u32[]{:S(2)}) copy-start(bf16[2048,8]{0,1:T(8,128)(2,1)} %param.28) | copy-start | bytes 98308
  19.5 6.3 %copy-start.15 = (f32[8]{0:T(128)S(1)}, f32[8]{0:T(128)}, u32[]{:S(2)}) copy-start(f32[8]{0:T(128)} %param.30) | copy-start | bytes 100
  20.6 5.3 %copy-start.10 = (f32[32,2]{0,1:T(2,128)S(1)}, f32[32,2]{0,1:T(2,128)}, u32[]{:S(2)}) copy-start(f32[32,2]{0,1:T(2,128)} %param.34) | copy-start | bytes 772
  20.9 18.1 %copy-start.5 = (f32[32,2,128]{2,1,0:T(2,128)S(1)}, f32[32,2,128]{2,1,0:T(2,128)}, u32[]{:S(2)}) copy-start(f32[32,2,128]{2,1,0:T(2,128)} %param.33) | copy-start | bytes 98308
  21.9 16.8 %all-to-all-start.1 = ((bf16[8,32,1024]{2,1,0:T(8,128)(2,1)}), bf16[8,32,1024]{2,1,0:T(8,128)(2,1)S(1)}, u32[]{:S(2)}, u32[]{:S(2)}) async-start(bf16[8,32,1024]{2,1,0:T(8,128)(2,1)} %bitcast.2), calls=%async_computation.1 | async-start | bytes 1048576 | tf_op jit(solution)/shard_map/all_to_all | solution.py:162
  26.0 17.5 %copy-start.9 = (f32[32,2]{0,1:T(2,128)}, f32[32,2]{0,1:T(2,128)S(1)}, u32[]{:S(2)}) copy-start(f32[32,2]{0,1:T(2,128)S(1)} %get-tuple-element.8) | copy-start | bytes 772
  45.7 24.8 %copy-start.7 = (bf16[2048]{0:T(1024)(128)(2,1)S(1)}, bf16[2048]{0:T(1024)(128)(2,1)}, u32[]{:S(2)}) copy-start(bf16[2048]{0:T(1024)(128)(2,1)} %param.22) | copy-start | bytes 12292
  46.0 1.9 %collective-permute-start = (bf16[32,512]{1,0:T(8,128)(2,1)S(1)}, bf16[32,512]{1,0:T(8,128)(2,1)S(1)}, u32[]{:S(2)}, u32[]{:S(2)}) collective-permute-start(bf16[32,512]{1,0:T(8,128)(2,1)S(1)} %get-tuple-element.13), channel_id=1, source_target_pairs={{0,1},{1,0},{2,3},{3,2},{4,5},{5,4},{6,7},{7,6},{8,9},{9,8},{10,11... | collective-permute-start | bytes 98312 | tf_op jit(solution)/shard_map/ppermute | solution.py:67
  46.1 4.0 %collective-permute-start.1 = (bf16[32,512]{1,0:T(8,128)(2,1)S(1)}, bf16[32,512]{1,0:T(8,128)(2,1)S(1)}, u32[]{:S(2)}, u32[]{:S(2)}) collective-permute-start(bf16[32,512]{1,0:T(8,128)(2,1)S(1)} %get-tuple-element.15), channel_id=1, source_target_pairs={{0,2},{1,3},{2,0},{3,1},{4,6},{5,7},{6,4},{7,5},{8,10},{9,11},{10,... | collective-permute-start | bytes 98312 | tf_op jit(solution)/shard_map/ppermute | solution.py:67
  47.6 3.4 %collective-permute-start.2 = (bf16[32,512]{1,0:T(8,128)(2,1)S(1)}, bf16[32,512]{1,0:T(8,128)(2,1)S(1)}, u32[]{:S(2)}, u32[]{:S(2)}) collective-permute-start(bf16[32,512]{1,0:T(8,128)(2,1)S(1)} %get-tuple-element.14), channel_id=1, source_target_pairs={{0,3},{1,2},{2,1},{3,0},{4,7},{5,6},{6,5},{7,4},{8,11},{9,10},{10,... | collective-permute-start | bytes 98312 | tf_op jit(solution)/shard_map/ppermute | solution.py:67
  63.7 6.6 %collective-permute-start.3 = (bf16[1,256,512]{2,1,0:T(8,128)(2,1)S(1)}, bf16[1,256,512]{2,1,0:T(8,128)(2,1)S(1)}, u32[]{:S(2)}, u32[]{:S(2)}) collective-permute-start(bf16[1,256,512]{2,1,0:T(8,128)(2,1)S(1)} %bitcast.123), channel_id=1, source_target_pairs={{0,2},{1,3},{2,0},{3,1},{4,6},{5,7},{6,4},{7,5},{8,10},{9,11},{10,... | collective-permute-start | bytes 786440 | tf_op jit(solution)/shard_map/ppermute | solution.py:67
  70.4 2.7 %collective-permute-start.4 = (bf16[2,256,512]{2,1,0:T(8,128)(2,1)S(1)}, bf16[2,256,512]{2,1,0:T(8,128)(2,1)S(1)}, u32[]{:S(2)}, u32[]{:S(2)}) collective-permute-start(bf16[2,256,512]{2,1,0:T(8,128)(2,1)S(1)} %maximum_bitcast_fusion), channel_id=1, source_target_pairs={{0,1},{1,0},{2,3},{3,2},{4,5},{5,4},{6,7},{7,6},{8,9},{9,8},{10,11... | collective-permute-start | bytes 1572872 | tf_op jit(solution)/shard_map/ppermute | solution.py:67
  84.3 2.1 %collective-permute-start.5 = (bf16[256,2,512]{2,0,1:T(8,128)(2,1)S(1)}, bf16[256,2,512]{2,0,1:T(8,128)(2,1)S(1)}, u32[]{:S(2)}, u32[]{:S(2)}) collective-permute-start(bf16[256,2,512]{2,0,1:T(8,128)(2,1)S(1)} %fusion.23), channel_id=1, source_target_pairs={{0,1},{1,0},{2,3},{3,2},{4,5},{5,4},{6,7},{7,6},{8,9},{9,8},{10,11... | collective-permute-start | bytes 1572872 | tf_op jit(solution)/shard_map/ppermute | solution.py:67
  88.3 14.3 %copy-start.8 = (f32[32,2]{0,1:T(2,128)S(1)}, f32[32,2]{0,1:T(2,128)}, u32[]{:S(2)}) copy-start(f32[32,2]{0,1:T(2,128)} %param.36) | copy-start | bytes 772
  88.3 14.3 %copy-start.11 = (s32[32,2]{0,1:T(2,128)S(1)}, s32[32,2]{0,1:T(2,128)}, u32[]{:S(2)}) copy-start(s32[32,2]{0,1:T(2,128)} %param.35) | copy-start | bytes 772
  88.3 8.7 %collective-permute-start.6 = (bf16[256,1,512]{2,0,1:T(8,128)(2,1)S(1)}, bf16[256,1,512]{2,0,1:T(8,128)(2,1)S(1)}, u32[]{:S(2)}, u32[]{:S(2)}) collective-permute-start(bf16[256,1,512]{2,0,1:T(8,128)(2,1)S(1)} %fusion.33), channel_id=1, source_target_pairs={{0,2},{1,3},{2,0},{3,1},{4,6},{5,7},{6,4},{7,5},{8,10},{9,11},{10,... | collective-permute-start | bytes 786440 | tf_op jit(solution)/shard_map/ppermute | solution.py:67
  97.8 13.3 %all-to-all-start.3 = ((bf16[8,32,512]{2,1,0:T(8,128)(2,1)}), bf16[8,32,512]{2,1,0:T(8,128)(2,1)S(1)}, u32[]{:S(2)}, u32[]{:S(2)}) async-start(bf16[8,32,512]{2,1,0:T(8,128)(2,1)} %bitcast.31), calls=%async_computation.3 | async-start | bytes 524288 | tf_op jit(solution)/shard_map/all_to_all | solution.py:224
  (2 other events, 4.2 us)
where the time goes:
time: 113 us; the launch traced here: 112 us
  waiting for transfers between devices  44.6 us (39%)
  starting transfers between devices  19.9 us (18%)
  other arithmetic  13.7 us (12%)
  matrix products  12.7 us (11%)
  blocking collectives  12.7 us (11%)
  local copies, waits for them, and re-layouts  7.19 us (6%)
    ppermute x7, waiting for transfers between devices, swap(): return lax.ppermute(value, axis, [(i, i ^ bit) for i in range(count)])  18 us
    all_to_all x1, blocking collectives, body(): lax.all_to_all(outgoing.reshape(ep_count * capacity, col_width), 'ep', sp...  12.7 us
    all_to_all x1, waiting for transfers between devices, body(): lax.all_to_all(terms, 'ep', split_axis=0, concat_axis=0, tiled=True)  12.5 us
    all_to_all x1, waiting for transfers between devices, body(): lax.all_to_all(half_share, 'ep', split_axis=0, concat_axis=0, tiled=True)  8.54 us
    all_to_all x1, starting transfers between devices, body(): lax.all_to_all(tokens, 'ep', split_axis=1, concat_axis=0, tiled=True)  7.31 us
    all_to_all x1, waiting for transfers between devices, body(): lax.all_to_all(tokens, 'ep', split_axis=1, concat_axis=0, tiled=True)  5.55 us
    all_to_all x1, starting transfers between devices, body(): lax.all_to_all(half_share, 'ep', split_axis=0, concat_axis=0, tiled=True)  4.7 us
    ppermute x7, starting transfers between devices, swap(): return lax.ppermute(value, axis, [(i, i ^ bit) for i in range(count)])  4.37 us
  transfers between devices with their start and end apart: 10, of which 8 were waited for; matrix products, arithmetic and copies ran while one was open for 5% of the time, Pallas kernels for 0%

commit v1 on v0

--- a/solution.py
+++ b/solution.py
@@ -4,6 +4,12 @@
 from jax.sharding import PartitionSpec as P
 
 norm_epsilon = 1e-06
+
+
+def trade_parts(block, name, split, join):
+    pieces = jnp.split(block, lax.axis_size(name), axis=split)
+    received = lax.all_to_all(jnp.stack(pieces), name, 0, 0)
+    return jnp.concatenate(received, axis=join)
 
 
 def rms_scale(row_block, gain):
@@ -149,7 +155,7 @@
     capacity = min(seq_dev, max(2, 2 * seq_dev * top_count // experts))
     every_row = capacity == seq_dev
     col_width = model_width // tp_count
-    foreign = lax.all_to_all(tokens, "ep", split_axis=1, concat_axis=0, tiled=True)
+    foreign = trade_parts(tokens, "ep", 1, 0)
     own_gain = lax.dynamic_slice_in_dim(gain_mix, ep_index * feature_rows, feature_rows, 0)
     scaled = (foreign.astype(jnp.float32) * own_gain.astype(jnp.float32)).astype(jnp.bfloat16)
     terms = jnp.concatenate(

time: 113 us -> 122 us (1.080)
  local copies, waits for them, and re-layouts: 7.19 us -> 16.2 us
    unnamed x32 -> x39, local copies, waits for them, and re-layouts: 0.1 us -> 9.52 us
    all_to_all x1 -> x0, local copies, waits for them, and re-layouts: 1.71 us -> none  [body(): lax.all_to_all(tokens, 'ep', split_axis=1, concat_axis=0, tiled=True)]
    another operation x0 -> x1, local copies, waits for them, and re-layouts: none -> 1.32 us  [trade_parts(): received = lax.all_to_all(jnp.stack(pieces), name, 0, 0)]
  transfers between devices with their start and end apart: 10 -> 10, of which waited for: 8 -> 8; matrix products, arithmetic and copies ran while one was open for 5% -> 4% of each run, Pallas kernels for 0% -> 0%
where the time goes in v1:
time: 122 us; the launch traced here: 121 us
  waiting for transfers between devices  44.6 us (37%)
  starting transfers between devices  19.9 us (16%)
  local copies, waits for them, and re-layouts  16.2 us (13%)
  other arithmetic  13.7 us (11%)
  matrix products  12.7 us (10%)
  blocking collectives  12.7 us (10%)
    ppermute x7, waiting for transfers between devices, swap(): return lax.ppermute(value, axis, [(i, i ^ bit) for i in range(count)])  18 us
    all_to_all x1, blocking collectives, body(): lax.all_to_all(outgoing.reshape(ep_count * capacity, col_width), 'ep', sp...  12.7 us
    all_to_all x1, waiting for transfers between devices, body(): lax.all_to_all(terms, 'ep', split_axis=0, concat_axis=0, tiled=True)  12.5 us
    unnamed x39, local copies, waits for them, and re-layouts  9.52 us
    all_to_all x1, waiting for transfers between devices, body(): lax.all_to_all(half_share, 'ep', split_axis=0, concat_axis=0, tiled=True)  8.54 us
    all_to_all x1, starting transfers between devices, trade_parts(): received = lax.all_to_all(jnp.stack(pieces), name, 0, 0)  7.31 us
    all_to_all x1, waiting for transfers between devices, trade_parts(): received = lax.all_to_all(jnp.stack(pieces), name, 0, 0)  5.55 us
    all_to_all x1, starting transfers between devices, body(): lax.all_to_all(half_share, 'ep', split_axis=0, concat_axis=0, tiled=True)  4.7 us
  transfers between devices with their start and end apart: 10, of which 8 were waited for; matrix products, arithmetic and copies ran while one was open for 4% of the time, Pallas kernels for 0%

profile of v1, /device:TPU:0, one launch (start us, length us, event | category | flops | bytes accessed | tf_op | source)
XLA Modules:
  0.0 120.9 jit_solution(13788117370893579399)
XLA Ops:
  0.7 1.5 %constant_dynamic-update-slice_fusion.7 = bf16[8,32,256]{2,1,0:T(8,128)(2,1)} fusion(bf16[32,2048]{1,0:T(8,128)(2,1)} %param.20), kind=kLoop, calls=%fused_computation.71 | loop fusion | bytes 32768
  2.1 1.3 %constant_dynamic-update-slice_fusion.6 = bf16[8,32,256]{2,1,0:T(8,128)(2,1)} fusion(bf16[8,32,256]{2,1,0:T(8,128)(2,1)} %constant_dynamic-update-slice_fusion.7, bf16[32,2048]{1,0:T(8,128)(2,1)} %param.20), kind=kLoop, calls=%fused_computation.70 | loop fusion | bytes 32768
  3.5 1.3 %constant_dynamic-update-slice_fusion.5 = bf16[8,32,256]{2,1,0:T(8,128)(2,1)} fusion(bf16[8,32,256]{2,1,0:T(8,128)(2,1)} %constant_dynamic-update-slice_fusion.6, bf16[32,2048]{1,0:T(8,128)(2,1)} %param.20), kind=kLoop, calls=%fused_computation.69 | loop fusion | bytes 32768
  10.1 1.3 %constant_dynamic-update-slice_fusion = bf16[8,32,256]{2,1,0:T(8,128)(2,1)} fusion(bf16[8,32,256]{2,1,0:T(8,128)(2,1)} %constant_dynamic-update-slice_fusion.1, bf16[32,2048]{1,0:T(8,128)(2,1)} %param.20), kind=kLoop, calls=%fused_computation.64 | loop fusion | bytes 32768 | tf_op jit(solution)/shard_map/stack | solution.py:11
  11.4 7.3 %all-to-all-start = ((bf16[8,32,256]{2,1,0:T(8,128)(2,1)}), bf16[8,32,256]{2,1,0:T(8,128)(2,1)S(1)}, u32[]{:S(2)}, u32[]{:S(2)}) async-start(bf16[8,32,256]{2,1,0:T(8,128)(2,1)} %constant_dynamic-update-slice_fusion), calls=%async_computation | async-start | bytes 262144 | tf_op jit(solution)/shard_map/all_to_all | solution.py:11
  20.5 5.6 %all-to-all-done = bf16[8,32,256]{2,1,0:T(8,128)(2,1)S(1)} async-done(((bf16[8,32,256]{2,1,0:T(8,128)(2,1)}), bf16[8,32,256]{2,1,0:T(8,128)(2,1)S(1)}, u32[]{:S(2)}, u32[]{:S(2)}) %all-to-all-start) | async-done | bytes 131104 | tf_op jit(solution)/shard_map/all_to_all | solution.py:11
  31.0 3.5 %all-to-all-start.1 = ((bf16[8,32,1024]{2,1,0:T(8,128)(2,1)}), bf16[8,32,1024]{2,1,0:T(8,128)(2,1)S(1)}, u32[]{:S(2)}, u32[]{:S(2)}) async-start(bf16[8,32,1024]{2,1,0:T(8,128)(2,1)} %bitcast.9), calls=%async_computation.1 | async-start | bytes 1048576 | tf_op jit(solution)/shard_map/all_to_all | solution.py:168
  35.3 12.5 %all-to-all-done.1 = bf16[8,32,1024]{2,1,0:T(8,128)(2,1)S(1)} async-done(((bf16[8,32,1024]{2,1,0:T(8,128)(2,1)}), bf16[8,32,1024]{2,1,0:T(8,128)(2,1)S(1)}, u32[]{:S(2)}, u32[]{:S(2)}) %all-to-all-start.1) | async-done | bytes 524320 | tf_op jit(solution)/shard_map/all_to_all | solution.py:168
  48.8 3.7 %multiply_add_fusion = f32[32,2,128,128]{3,2,1,0:T(8,128)S(1)} fusion(f32[32,2,128,128]{3,2,1,0:T(8,128)} %param.32, f32[32,2,128]{2,1,0:T(2,128)S(1)} %reshape.183, f32[32,2,128]{2,1,0:T(2,128)S(1)} %get-tuple-element.6, f32[32,2]{1,0:T(8,128)S(1)} %copy.48), kind=kLoop, calls=%fused_computation | loop fusion | flops 3145728 | bytes 8454400 | tf_op jit(solution)/shard_map/add | solution.py:39
  52.6 2.0 %fusion.48 = f32[32,2,1,128]{3,2,1,0:T(1,128)S(1)} fusion(bf16[32,2,128,1]{2,3,1,0:T(2,128)(2,1)S(1)} %reshape.192, f32[32,2,128,128]{3,2,1,0:T(8,128)S(1)} %multiply_add_fusion), kind=kOutput, calls=%fused_computation.95 | convolution fusion | flops 12582912 | bytes 4243456 | tf_op jit(solution)/shard_map/shd,shde->she/dot_general | solution.py:44
  55.1 1.6 %collective-permute-start.1 = (bf16[32,512]{1,0:T(8,128)(2,1)S(1)}, bf16[32,512]{1,0:T(8,128)(2,1)S(1)}, u32[]{:S(2)}, u32[]{:S(2)}) collective-permute-start(bf16[32,512]{1,0:T(8,128)(2,1)S(1)} %get-tuple-element.15), channel_id=1, source_target_pairs={{0,2},{1,3},{2,0},{3,1},{4,6},{5,7},{6,4},{7,5},{8,10},{9,11},{10,... | collective-permute-start | bytes 98312 | tf_op jit(solution)/shard_map/ppermute | solution.py:73
  57.0 2.1 %collective-permute-done.1 = bf16[32,512]{1,0:T(8,128)(2,1)S(1)} collective-permute-done((bf16[32,512]{1,0:T(8,128)(2,1)S(1)}, bf16[32,512]{1,0:T(8,128)(2,1)S(1)}, u32[]{:S(2)}, u32[]{:S(2)}) %collective-permute-start.1) | collective-permute-done | bytes 32800 | tf_op jit(solution)/shard_map/ppermute | solution.py:73
  60.1 12.7 %all_to_all.29 = bf16[8,32,512]{2,1,0:T(8,128)(2,1)S(1)} all-to-all(bf16[8,32,512]{2,1,0:T(8,128)(2,1)S(1)} %all_to_all.22), channel_id=1, replica_groups=mesh['ep'=8,'tp'=4] {'ep'}, dimensions={0} | all-to-all | bytes 524288 | tf_op jit(solution)/shard_map/all_to_all | solution.py:216
  73.7 5.7 %collective-permute-done.3 = bf16[1,256,512]{2,1,0:T(8,128)(2,1)S(1)} collective-permute-done((bf16[1,256,512]{2,1,0:T(8,128)(2,1)S(1)}, bf16[1,256,512]{2,1,0:T(8,128)(2,1)S(1)}, u32[]{:S(2)}, u32[]{:S(2)}) %collective-permute-start.3) | collective-permute-done | bytes 262176 | tf_op jit(solution)/shard_map/ppermute | solution.py:73
  79.6 2.6 %copy.61 = bf16[2048,384]{1,0:T(8,128)(2,1)} copy(bf16[2048,384]{0,1:T(8,128)(2,1)} %bitcast.130) | data formatting | bytes 3145728 | tf_op jit(solution)/shard_map/dot_general | solution.py:228
  84.0 1.5 %copy.52 = bf16[256,4,512]{0,2,1:T(8,128)(2,1)S(1)} copy(bf16[256,4,512]{2,0,1:T(8,128)(2,1)} %fusion.16) | data formatting | bytes 2097152 | tf_op jit(solution)/shard_map/convert_element_type | solution.py:18
  85.5 2.1 %fusion.5 = f32[256,384]{1,0:T(8,128)S(1)} fusion(bf16[256,2048]{0,1:T(8,128)(2,1)S(1)} %bitcast.128, bf16[1,2048,384]{2,1,0:T(8,128)(2,1)} %param.37), kind=kOutput, calls=%fused_computation.8 | convolution fusion | flops 402653184 | bytes 3014656 | tf_op jit(solution)/shard_map/dot_general | solution.py:225
  87.6 4.1 %fusion.21 = f32[256,2,2,512]{3,0,2,1:T(8,128)} fusion(bf16[2,2,512,384]{3,2,1,0:T(8,128)(2,1)} %bitcast.131, bf16[256,2048]{0,1:T(8,128)(2,1)S(1)} %bitcast.129, bf16[1,2048,384]{2,1,0:T(8,128)(2,1)S(1)} %copy-done, f32[256,384]{1,0:T(8,128)S(1)} %fusion.5), kind=kOutput, calls=%fused_computation.27 | convolution fusion | flops 805896192 | bytes 6684672 | tf_op jit(solution)/shard_map/dot_general | solution.py:228
  91.8 1.6 %fusion.23 = bf16[256,2,512]{2,0,1:T(8,128)(2,1)S(1)} fusion(f32[256,2,2,512]{3,0,2,1:T(8,128)} %fusion.21, pred[]{:T(512)S(6)} %eq.29), kind=kLoop, calls=%fused_computation.28 | loop fusion | flops 262144 | bytes 1572865 | tf_op jit(solution)/shard_map/convert_element_type | solution.py:103
  93.9 1.5 %collective-permute-done.5 = bf16[256,2,512]{2,0,1:T(8,128)(2,1)S(1)} collective-permute-done((bf16[256,2,512]{2,0,1:T(8,128)(2,1)S(1)}, bf16[256,2,512]{2,0,1:T(8,128)(2,1)S(1)}, u32[]{:S(2)}, u32[]{:S(2)}) %collective-permute-start.5) | collective-permute-done | bytes 524320 | tf_op jit(solution)/shard_map/ppermute | solution.py:73
  95.5 1.8 %fusion.19 = f32[256,1,2,512]{3,0,2,1:T(8,128)S(1)} fusion(bf16[256,2,512]{2,0,1:T(8,128)(2,1)S(1)} %collective-permute-done.5, f32[256,2,2,512]{3,0,2,1:T(8,128)} %fusion.21, pred[]{:T(512)S(6)} %eq.29), kind=kLoop, calls=%fused_computation.24 | loop fusion | flops 786432 | bytes 3670017 | tf_op jit(solution)/shard_map/reshape | solution.py:100
  98.4 7.7 %collective-permute-done.6 = bf16[256,1,512]{2,0,1:T(8,128)(2,1)S(1)} collective-permute-done((bf16[256,1,512]{2,0,1:T(8,128)(2,1)S(1)}, bf16[256,1,512]{2,0,1:T(8,128)(2,1)S(1)}, u32[]{:S(2)}, u32[]{:S(2)}) %collective-permute-start.6) | collective-permute-done | bytes 262176 | tf_op jit(solution)/shard_map/ppermute | solution.py:73
  106.9 4.7 %all-to-all-start.3 = ((bf16[8,32,512]{2,1,0:T(8,128)(2,1)}), bf16[8,32,512]{2,1,0:T(8,128)(2,1)S(1)}, u32[]{:S(2)}, u32[]{:S(2)}) async-start(bf16[8,32,512]{2,1,0:T(8,128)(2,1)} %bitcast.38), calls=%async_computation.3 | async-start | bytes 524288 | tf_op jit(solution)/shard_map/all_to_all | solution.py:230
  111.7 8.5 %all-to-all-done.3 = bf16[8,32,512]{2,1,0:T(8,128)(2,1)S(1)} async-done(((bf16[8,32,512]{2,1,0:T(8,128)(2,1)}), bf16[8,32,512]{2,1,0:T(8,128)(2,1)S(1)}, u32[]{:S(2)}, u32[]{:S(2)}) %all-to-all-start.3) | async-done | bytes 262176 | tf_op jit(solution)/shard_map/all_to_all | solution.py:230
  (94 shorter events, 21.4 us)
Async XLA Ops:
  0.6 87.0 %copy-start = (bf16[1,2048,384]{2,1,0:T(8,128)(2,1)S(1)}, bf16[1,2048,384]{2,1,0:T(8,128)(2,1)}, u32[]{:S(2)}) copy-start(bf16[1,2048,384]{2,1,0:T(8,128)(2,1)} %param.38) | copy-start | bytes 4718596
  0.6 29.0 %copy-start.4 = (bf16[256,256]{1,0:T(8,128)(2,1)S(1)}, bf16[256,256]{1,0:T(8,128)(2,1)}, u32[]{:S(2)}) copy-start(bf16[256,256]{1,0:T(8,128)(2,1)} %param.23) | copy-start | bytes 393220
  11.4 14.7 %all-to-all-start = ((bf16[8,32,256]{2,1,0:T(8,128)(2,1)}), bf16[8,32,256]{2,1,0:T(8,128)(2,1)S(1)}, u32[]{:S(2)}, u32[]{:S(2)}) async-start(bf16[8,32,256]{2,1,0:T(8,128)(2,1)} %constant_dynamic-update-slice_fusion), calls=%async_computation | async-start | bytes 262144 | tf_op jit(solution)/shard_map/all_to_all | solution.py:11
  27.2 7.3 %copy-start.6 = (bf16[2048]{0:T(1024)(128)(2,1)S(1)}, bf16[2048]{0:T(1024)(128)(2,1)}, u32[]{:S(2)}) copy-start(bf16[2048]{0:T(1024)(128)(2,1)} %param.21) | copy-start | bytes 12292
  27.2 7.3 %copy-start.3 = (bf16[32,2048]{1,0:T(8,128)(2,1)S(1)}, bf16[32,2048]{1,0:T(8,128)(2,1)}, u32[]{:S(2)}) copy-start(bf16[32,2048]{1,0:T(8,128)(2,1)} %param.20) | copy-start | bytes 393220
  27.3 7.3 %copy-start.12 = (bf16[2048,8]{0,1:T(8,128)(2,1)S(1)}, bf16[2048,8]{0,1:T(8,128)(2,1)}, u32[]{:S(2)}) copy-start(bf16[2048,8]{0,1:T(8,128)(2,1)} %param.27) | copy-start | bytes 98308
  27.3 7.3 %copy-start.14 = (f32[8]{0:T(128)S(1)}, f32[8]{0:T(128)}, u32[]{:S(2)}) copy-start(f32[8]{0:T(128)} %param.29) | copy-start | bytes 100
  28.5 6.3 %copy-start.13 = (bf16[2048,8]{0,1:T(8,128)(2,1)S(1)}, bf16[2048,8]{0,1:T(8,128)(2,1)}, u32[]{:S(2)}) copy-start(bf16[2048,8]{0,1:T(8,128)(2,1)} %param.28) | copy-start | bytes 98308
  28.5 6.3 %copy-start.15 = (f32[8]{0:T(128)S(1)}, f32[8]{0:T(128)}, u32[]{:S(2)}) copy-start(f32[8]{0:T(128)} %param.30) | copy-start | bytes 100
  29.7 5.3 %copy-start.10 = (f32[32,2]{0,1:T(2,128)S(1)}, f32[32,2]{0,1:T(2,128)}, u32[]{:S(2)}) copy-start(f32[32,2]{0,1:T(2,128)} %param.34) | copy-start | bytes 772
  30.0 18.1 %copy-start.5 = (f32[32,2,128]{2,1,0:T(2,128)S(1)}, f32[32,2,128]{2,1,0:T(2,128)}, u32[]{:S(2)}) copy-start(f32[32,2,128]{2,1,0:T(2,128)} %param.33) | copy-start | bytes 98308
  31.0 16.8 %all-to-all-start.1 = ((bf16[8,32,1024]{2,1,0:T(8,128)(2,1)}), bf16[8,32,1024]{2,1,0:T(8,128)(2,1)S(1)}, u32[]{:S(2)}, u32[]{:S(2)}) async-start(bf16[8,32,1024]{2,1,0:T(8,128)(2,1)} %bitcast.9), calls=%async_computation.1 | async-start | bytes 1048576 | tf_op jit(solution)/shard_map/all_to_all | solution.py:168
  35.0 17.5 %copy-start.9 = (f32[32,2]{0,1:T(2,128)}, f32[32,2]{0,1:T(2,128)S(1)}, u32[]{:S(2)}) copy-start(f32[32,2]{0,1:T(2,128)S(1)} %get-tuple-element.8) | copy-start | bytes 772
  54.7 24.9 %copy-start.7 = (bf16[2048]{0:T(1024)(128)(2,1)S(1)}, bf16[2048]{0:T(1024)(128)(2,1)}, u32[]{:S(2)}) copy-start(bf16[2048]{0:T(1024)(128)(2,1)} %param.22) | copy-start | bytes 12292
  55.0 1.9 %collective-permute-start = (bf16[32,512]{1,0:T(8,128)(2,1)S(1)}, bf16[32,512]{1,0:T(8,128)(2,1)S(1)}, u32[]{:S(2)}, u32[]{:S(2)}) collective-permute-start(bf16[32,512]{1,0:T(8,128)(2,1)S(1)} %get-tuple-element.13), channel_id=1, source_target_pairs={{0,1},{1,0},{2,3},{3,2},{4,5},{5,4},{6,7},{7,6},{8,9},{9,8},{10,11... | collective-permute-start | bytes 98312 | tf_op jit(solution)/shard_map/ppermute | solution.py:73
  55.1 4.0 %collective-permute-start.1 = (bf16[32,512]{1,0:T(8,128)(2,1)S(1)}, bf16[32,512]{1,0:T(8,128)(2,1)S(1)}, u32[]{:S(2)}, u32[]{:S(2)}) collective-permute-start(bf16[32,512]{1,0:T(8,128)(2,1)S(1)} %get-tuple-element.15), channel_id=1, source_target_pairs={{0,2},{1,3},{2,0},{3,1},{4,6},{5,7},{6,4},{7,5},{8,10},{9,11},{10,... | collective-permute-start | bytes 98312 | tf_op jit(solution)/shard_map/ppermute | solution.py:73
  56.7 3.4 %collective-permute-start.2 = (bf16[32,512]{1,0:T(8,128)(2,1)S(1)}, bf16[32,512]{1,0:T(8,128)(2,1)S(1)}, u32[]{:S(2)}, u32[]{:S(2)}) collective-permute-start(bf16[32,512]{1,0:T(8,128)(2,1)S(1)} %get-tuple-element.14), channel_id=1, source_target_pairs={{0,3},{1,2},{2,1},{3,0},{4,7},{5,6},{6,5},{7,4},{8,11},{9,10},{10,... | collective-permute-start | bytes 98312 | tf_op jit(solution)/shard_map/ppermute | solution.py:73
  72.8 6.6 %collective-permute-start.3 = (bf16[1,256,512]{2,1,0:T(8,128)(2,1)S(1)}, bf16[1,256,512]{2,1,0:T(8,128)(2,1)S(1)}, u32[]{:S(2)}, u32[]{:S(2)}) collective-permute-start(bf16[1,256,512]{2,1,0:T(8,128)(2,1)S(1)} %bitcast.132), channel_id=1, source_target_pairs={{0,2},{1,3},{2,0},{3,1},{4,6},{5,7},{6,4},{7,5},{8,10},{9,11},{10,... | collective-permute-start | bytes 786440 | tf_op jit(solution)/shard_map/ppermute | solution.py:73
  79.5 2.7 %collective-permute-start.4 = (bf16[2,256,512]{2,1,0:T(8,128)(2,1)S(1)}, bf16[2,256,512]{2,1,0:T(8,128)(2,1)S(1)}, u32[]{:S(2)}, u32[]{:S(2)}) collective-permute-start(bf16[2,256,512]{2,1,0:T(8,128)(2,1)S(1)} %maximum_bitcast_fusion), channel_id=1, source_target_pairs={{0,1},{1,0},{2,3},{3,2},{4,5},{5,4},{6,7},{7,6},{8,9},{9,8},{10,11... | collective-permute-start | bytes 1572872 | tf_op jit(solution)/shard_map/ppermute | solution.py:73
  93.4 2.1 %collective-permute-start.5 = (bf16[256,2,512]{2,0,1:T(8,128)(2,1)S(1)}, bf16[256,2,512]{2,0,1:T(8,128)(2,1)S(1)}, u32[]{:S(2)}, u32[]{:S(2)}) collective-permute-start(bf16[256,2,512]{2,0,1:T(8,128)(2,1)S(1)} %fusion.23), channel_id=1, source_target_pairs={{0,1},{1,0},{2,3},{3,2},{4,5},{5,4},{6,7},{7,6},{8,9},{9,8},{10,11... | collective-permute-start | bytes 1572872 | tf_op jit(solution)/shard_map/ppermute | solution.py:73
  97.3 14.3 %copy-start.8 = (f32[32,2]{0,1:T(2,128)S(1)}, f32[32,2]{0,1:T(2,128)}, u32[]{:S(2)}) copy-start(f32[32,2]{0,1:T(2,128)} %param.36) | copy-start | bytes 772
  97.3 14.3 %copy-start.11 = (s32[32,2]{0,1:T(2,128)S(1)}, s32[32,2]{0,1:T(2,128)}, u32[]{:S(2)}) copy-start(s32[32,2]{0,1:T(2,128)} %param.35) | copy-start | bytes 772
  97.4 8.7 %collective-permute-start.6 = (bf16[256,1,512]{2,0,1:T(8,128)(2,1)S(1)}, bf16[256,1,512]{2,0,1:T(8,128)(2,1)S(1)}, u32[]{:S(2)}, u32[]{:S(2)}) collective-permute-start(bf16[256,1,512]{2,0,1:T(8,128)(2,1)S(1)} %fusion.33), channel_id=1, source_target_pairs={{0,2},{1,3},{2,0},{3,1},{4,6},{5,7},{6,4},{7,5},{8,10},{9,11},{10,... | collective-permute-start | bytes 786440 | tf_op jit(solution)/shard_map/ppermute | solution.py:73
  106.9 13.3 %all-to-all-start.3 = ((bf16[8,32,512]{2,1,0:T(8,128)(2,1)}), bf16[8,32,512]{2,1,0:T(8,128)(2,1)S(1)}, u32[]{:S(2)}, u32[]{:S(2)}) async-start(bf16[8,32,512]{2,1,0:T(8,128)(2,1)} %bitcast.38), calls=%async_computation.3 | async-start | bytes 524288 | tf_op jit(solution)/shard_map/all_to_all | solution.py:230
  (2 other events, 4.2 us)
